TPU v7x, 32 devices: a whole 2x2x4 slice. The times are simulated.
32 devices in a mesh: sp: 8 (over z, core), tp: 4 (over y, x).
Axes of the slice: x: 2, y: 2, z: 4, core: 2. Of those that a mesh axis runs over, the one named last changes fastest.
Arguments:
- moe_input: bfloat16 [2048, 2048], P('sp', 'tp'), may hold values from -6 to 6
- out_grad: bfloat16 [2048, 2048], P('sp', 'tp'), may hold values from -8 to 8
- routes: int32 [2048, 2], P('sp'), may hold values from 0 to 7, all different within a row; in each aligned block of 256 rows (0 to 255, 256 to 511, ...) at most 80 rows name the same one
- route_weight: float32 [2048, 2], P('sp'), may hold values from 0.2 to 1.5
- w_gate: bfloat16 [8, 2048, 2048], P('sp', None, 'tp'), may hold values from -0.125 to 0.125
- w_up: bfloat16 [8, 2048, 2048], P('sp', None, 'tp'), may hold values from -0.125 to 0.125
- w_down: bfloat16 [8, 2048, 2048], P('sp', 'tp'), may hold values from -0.125 to 0.125
- w_out: bfloat16 [2048, 2048], P(None, 'tp'), may hold values from -0.125 to 0.125
- queries: bfloat16 [2048, 1024], P('sp', 'tp'), may hold values from -6 to 6
- key_rows: bfloat16 [2048, 1024], P('sp', 'tp'), may hold values from -6 to 6
- value_rows: bfloat16 [2048, 2048], P('sp', 'tp'), may hold values from -6 to 6
- log_decay: float32 [2048, 1024], P('sp', 'tp'), may hold values from -1 to 0
Outputs:
- grad_gate: bfloat16 [8, 2048, 2048], P('sp', None, 'tp')
- grad_up: bfloat16 [8, 2048, 2048], P('sp', None, 'tp')
- grad_down: bfloat16 [8, 2048, 2048], P('sp', 'tp')
- grad_proj: float32 [2048, 2048], P('sp', 'tp')
- grad_queries: bfloat16 [2048, 1024], P('sp', 'tp')
- grad_keys: bfloat16 [2048, 1024], P('sp', 'tp')
- grad_values: bfloat16 [2048, 2048], P('sp', 'tp')
- grad_decay: float32 [2048, 1024], P('sp', 'tp')
Inputs may be any that keep to these rules, and one draw needn't show every extreme that they name: `routes`: A token's experts differ. Within each aligned block of 256 tokens no expert is named more than 80 times, and in some block one expert is named exactly 80 times.
All inputs are finite; a program needn't handle non-finite values.
Results may differ from a plain program's by a relative error of at most 0.025.
Values may be sent and summed in bfloat16 or wider, within the bound.
A program may use at most 64 MiB of HBM per device.

v0:
```python
import jax
import jax.numpy as jnp
from jax import lax
from jax.sharding import PartitionSpec as P

KEY_CHANNELS = 32
VAL_DIM = 64
TOP = 2
BLOCK = 64
PRECISE = lax.Precision.HIGHEST


def carried_in(value, axis, join, neutral, backward):
    count, mine = (lax.axis_size(axis), lax.axis_index(axis))
    pieces = jax.tree.map(lambda part: lax.all_gather(part, axis), value)
    if backward:
        pieces = jax.tree.map(lambda part: part[::-1], pieces)
        mine = count - 1 - mine
    subtotal = jax.tree.map(
        lambda part, zero: jnp.full_like(part, 0) + jnp.asarray(zero, part.dtype), value, neutral
    )

    def hop(position, subtotal):
        longer = join(subtotal, jax.tree.map(lambda part: part[position], pieces))
        return jax.tree.map(lambda new, old: jnp.where(position < mine, new, old), longer, subtotal)

    return lax.fori_loop(0, count - 1, hop, subtotal)


def mixer_pass(queries, key_rows, value_rows, log_decay, state_in):
    length = queries.shape[0]
    blocks = length // BLOCK
    nheads = state_in.shape[0]
    query_blocks = queries.reshape(blocks, BLOCK, nheads, KEY_CHANNELS)
    key_blocks = key_rows.reshape(blocks, BLOCK, nheads, KEY_CHANNELS) * KEY_CHANNELS ** (-0.5)
    value_blocks = value_rows.reshape(blocks, BLOCK, nheads, VAL_DIM)
    decays = log_decay.reshape(blocks, BLOCK, nheads, KEY_CHANNELS)
    cumulative = jnp.cumsum(decays, axis=1)
    closing = cumulative[:, -1]
    query_scaled = query_blocks * jnp.exp(cumulative)
    key_scaled = key_blocks * jnp.exp(-cumulative)
    causal = jnp.tril(jnp.ones((BLOCK, BLOCK), jnp.float32))
    scores = jnp.einsum("nthd,nshd->nhts", query_scaled, key_scaled, precision=PRECISE) * causal
    within = jnp.einsum("nhts,nshv->nthv", scores, value_blocks, precision=PRECISE)
    key_tail = key_blocks * jnp.exp(closing[:, None] - cumulative)
    additions = jnp.einsum("nshd,nshv->nhdv", key_tail, value_blocks, precision=PRECISE)

    def advance(state_now, pieces):
        return (jnp.exp(pieces[0])[..., None] * state_now + pieces[1], state_now)

    state_out, entering = lax.scan(advance, state_in, (closing, additions))
    carried = jnp.einsum("nthd,nhdv->nthv", query_scaled, entering, precision=PRECISE)
    return (within + carried).reshape(length, nheads * VAL_DIM)


def carry_terms(key_full, value_full, decay_full):
    length = key_full.shape[0]
    blocks = length // BLOCK
    nheads = key_full.shape[1] // KEY_CHANNELS
    key_blocks = key_full.reshape(blocks, BLOCK, nheads, KEY_CHANNELS) * KEY_CHANNELS ** (-0.5)
    value_blocks = value_full.reshape(blocks, BLOCK, nheads, VAL_DIM)
    cumulative = jnp.cumsum(decay_full.reshape(blocks, BLOCK, nheads, KEY_CHANNELS), axis=1)
    closing = cumulative[:, -1]
    key_tail = key_blocks * jnp.exp(closing[:, None] - cumulative)
    additions = jnp.einsum("nshd,nshv->nhdv", key_tail, value_blocks, precision=PRECISE)
    log_total = jnp.sum(closing, axis=0)
    remaining = log_total[None] - jnp.cumsum(closing, axis=0)
    increment = jnp.einsum("nhd,nhdv->hdv", jnp.exp(remaining), additions, precision=PRECISE)
    return (log_total, increment)


def chain_step(earlier, latter):
    return (earlier[0] + latter[0], jnp.exp(latter[0])[..., None] * earlier[1] + latter[1])


def body(
    moe_input,
    out_grad,
    routes,
    route_weight,
    w_gate,
    w_up,
    w_down,
    w_out,
    queries,
    key_rows,
    value_rows,
    log_decay,
):
    sp_count = lax.axis_size("sp")
    token_count = out_grad.shape[0]
    pair_count = token_count * TOP
    capacity = 5 * token_count * TOP // (4 * sp_count)
    query_full = queries.astype(jnp.float32)
    key_full = key_rows.astype(jnp.float32)
    value_full = value_rows.astype(jnp.float32)
    (log_total, increment), pull_carry = jax.vjp(carry_terms, key_full, value_full, log_decay)
    state_in = carried_in(
        (log_total, increment),
        "sp",
        chain_step,
        (jnp.zeros_like(log_total), jnp.zeros_like(increment)),
        False,
    )[1]
    mixer_raw, pull_mixer = jax.vjp(
        mixer_pass, query_full, key_full, value_full, log_decay, state_in
    )
    mixer_out = mixer_raw.astype(jnp.bfloat16)
    flat_routes = routes.reshape(pair_count)
    onehot = (flat_routes[:, None] == jnp.arange(sp_count, dtype=jnp.int32)[None, :]).astype(
        jnp.int32
    )
    position = jnp.sum((jnp.cumsum(onehot, axis=0) - onehot) * onehot, axis=1)
    pair_slot = flat_routes * capacity + position
    slot_pair = (
        jnp.full((sp_count * capacity,), pair_count, jnp.int32)
        .at[pair_slot]
        .set(jnp.arange(pair_count, dtype=jnp.int32))
    )
    slot_token = slot_pair // TOP
    row_total = sp_count * capacity
    columns = out_grad.shape[1]
    weighted = (route_weight[:, :, None] * out_grad[:, None, :].astype(jnp.float32)).astype(
        jnp.bfloat16
    )
    weighted_pad = jnp.concatenate(
        [weighted.reshape(pair_count, columns), jnp.zeros((1, columns), jnp.bfloat16)], axis=0
    )
    inputs_pad = jnp.concatenate([moe_input, jnp.zeros((1, columns), jnp.bfloat16)], axis=0)
    send_in = jnp.take(inputs_pad, slot_token, axis=0).reshape(sp_count, capacity, columns)
    send_grad = jnp.take(weighted_pad, slot_pair, axis=0).reshape(sp_count, capacity, columns)
    send_in, send_grad = (send_in, send_grad)
    recv_in, recv_grad = (
        lax.all_to_all(send_in, "sp", split_axis=0, concat_axis=0, tiled=True),
        lax.all_to_all(send_grad, "sp", split_axis=0, concat_axis=0, tiled=True),
    )
    rows_in, rows_grad = (
        lax.all_gather(recv_in.reshape(row_total, -1), "tp", axis=1, tiled=True),
        lax.all_gather(recv_grad.reshape(row_total, -1), "tp", axis=1, tiled=True),
    )
    gate_weight = w_gate[0]
    up_weight = w_up[0]
    down_weight = w_down[0]
    gate_pre = jnp.dot(rows_in, gate_weight, preferred_element_type=jnp.float32)
    up_pre = jnp.dot(rows_in, up_weight, preferred_element_type=jnp.float32)
    sigmoid_gate = jax.nn.sigmoid(gate_pre)
    activated = gate_pre * sigmoid_gate
    hidden = (activated * up_pre).astype(jnp.bfloat16)
    hidden_grad = lax.dot_general(
        rows_grad, down_weight, (((1,), (1,)), ((), ())), preferred_element_type=jnp.float32
    )
    down_part = lax.dot_general(
        hidden, rows_grad, (((0,), (0,)), ((), ())), preferred_element_type=jnp.float32
    ).astype(jnp.bfloat16)
    gate_grad = (
        hidden_grad * up_pre * sigmoid_gate * (1.0 + gate_pre * (1.0 - sigmoid_gate))
    ).astype(jnp.bfloat16)
    up_grad = (hidden_grad * activated).astype(jnp.bfloat16)
    gate_part = lax.dot_general(
        rows_in, gate_grad, (((0,), (0,)), ((), ())), preferred_element_type=jnp.float32
    ).astype(jnp.bfloat16)
    up_part = lax.dot_general(
        rows_in, up_grad, (((0,), (0,)), ((), ())), preferred_element_type=jnp.float32
    ).astype(jnp.bfloat16)
    partial_value = lax.dot_general(
        gate_grad, gate_weight, (((1,), (1,)), ((), ())), preferred_element_type=jnp.float32
    )
    partial_value = partial_value + lax.dot_general(
        up_grad, up_weight, (((1,), (1,)), ((), ())), preferred_element_type=jnp.float32
    )
    row_part = lax.psum_scatter(
        partial_value.astype(jnp.bfloat16), "tp", scatter_dimension=1, tiled=True
    )
    back_rows = lax.all_to_all(
        row_part.reshape(sp_count, capacity, -1), "sp", split_axis=0, concat_axis=0, tiled=True
    ).reshape(row_total, -1)
    routed = jnp.sum(
        jnp.take(back_rows, pair_slot, axis=0).astype(jnp.float32).reshape(token_count, TOP, -1),
        axis=1,
    )
    residual_grad = (out_grad.astype(jnp.float32) + routed).astype(jnp.bfloat16)
    full_grad = lax.all_gather(residual_grad, "tp", axis=1, tiled=True)
    grad_proj = lax.psum_scatter(
        lax.dot_general(
            full_grad, mixer_out, (((0,), (0,)), ((), ())), preferred_element_type=jnp.float32
        ).astype(jnp.bfloat16),
        "sp",
        scatter_dimension=0,
        tiled=True,
    ).astype(jnp.float32)
    mixer_grad = jnp.dot(full_grad, w_out, preferred_element_type=jnp.float32)
    query_grad, key_grad, value_grad, decay_grad, state_grad = pull_mixer(mixer_grad)
    state_out_grad = carried_in(
        (log_total, state_grad),
        "sp",
        chain_step,
        (jnp.zeros_like(log_total), jnp.zeros_like(state_grad)),
        True,
    )[1]
    total_grad = jnp.exp(log_total) * jnp.sum(state_out_grad * state_in, axis=2)
    key_extra, value_extra, decay_extra = pull_carry((total_grad, state_out_grad))
    return (
        gate_part[None],
        up_part[None],
        down_part[None],
        grad_proj,
        query_grad.astype(jnp.bfloat16),
        (key_grad + key_extra).astype(jnp.bfloat16),
        (value_grad + value_extra).astype(jnp.bfloat16),
        decay_grad + decay_extra,
    )


def solution(mesh):
    in_specs = (
        P("sp", "tp"),
        P("sp", "tp"),
        P("sp", None),
        P("sp", None),
        P("sp", None, "tp"),
        P("sp", None, "tp"),
        P("sp", "tp", None),
        P(None, "tp"),
        P("sp", "tp"),
        P("sp", "tp"),
        P("sp", "tp"),
        P("sp", "tp"),
    )
    out_specs = (
        P("sp", None, "tp"),
        P("sp", None, "tp"),
        P("sp", "tp", None),
        P("sp", "tp"),
        P("sp", "tp"),
        P("sp", "tp"),
        P("sp", "tp"),
        P("sp", "tp"),
    )
    return jax.shard_map(body, mesh=mesh, in_specs=in_specs, out_specs=out_specs, check_vma=False)
```

profile of v0, /device:TPU:0, one launch (start us, length us, event | category | flops | bytes accessed | tf_op | source)
XLA Modules:
  0.0 410.4 jit_solution(14217362036748022045)
XLA Ops:
  18.1 24.4 %all_to_all.15 = bf16[8,80,512]{2,1,0:T(8,128)(2,1)} all-to-all(bf16[8,80,512]{2,1,0:T(8,128)(2,1)S(1)} %broadcast_select_fusion.2), channel_id=1, replica_groups=mesh['sp'=8,'tp'=4] {'sp'}, dimensions={0} | all-to-all | bytes 1310720 | tf_op jit(solution)/shard_map/all_to_all | solution.py:134
  49.3 21.2 %all_to_all.16 = bf16[8,80,512]{2,1,0:T(8,128)(2,1)} all-to-all(bf16[8,80,512]{2,1,0:T(8,128)(2,1)S(1)} %broadcast_select_fusion.1), channel_id=1, replica_groups=mesh['sp'=8,'tp'=4] {'sp'}, dimensions={0} | all-to-all | bytes 1310720 | tf_op jit(solution)/shard_map/all_to_all | solution.py:135
  71.1 9.8 %all-gather.7.cloned.1.call-done = bf16[640,2048]{1,0:T(8,128)(2,1)} async-done(((bf16[640,512]{1,0:T(8,128)(2,1)}), bf16[640,2048]{1,0:T(8,128)(2,1)}) %all-gather.7.cloned.1.call-update) | async-done | bytes 2621456 | tf_op jit(solution)/shard_map/all_gather | solution.py:138
  81.0 3.4 fusion.11
  87.0 35.2 %all-gather.9.cloned.1.call-done = bf16[640,2048]{1,0:T(8,128)(2,1)} async-done(((bf16[640,512]{1,0:T(8,128)(2,1)}), bf16[640,2048]{1,0:T(8,128)(2,1)}) %all-gather.9.cloned.1.call-update) | async-done | bytes 2621456 | tf_op jit(solution)/shard_map/all_gather | solution.py:139
  122.2 4.6 %multiply_convert_fusion.1 = (bf16[640,512]{1,0:T(8,128)(2,1)S(1)}, bf16[640,512]{1,0:T(8,128)(2,1)S(1)}) fusion(f32[640,512]{1,0:T(8,128)S(1)} %fusion.11, f32[640,512]{1,0:T(8,128)} %fusion.14, bf16[640,2048]{1,0:T(8,128)(2,1)} %all-gather.9.cloned.1.call-done, bf16[1,512,2048]{2,1,0:T(8,128)(2,1)} %param.26), kind=kOutput, calls=%fused_computation.48 | convolution fusion | flops 1346437120 | bytes 8650752 | tf_op jit(solution)/shard_map/dot_general | solution.py:149
  128.9 3.1 add_convert_fusion
  133.6 25.9 %fusion.66 = f32[4,64,8,32]{3,2,1,0:T(8,128)S(1)} fusion(f32[4,64,8,32]{3,2,1,0:T(8,128)S(1)} %reshape.284), kind=kOutput, calls=%fused_computation.146 | output fusion | flops 4128768 | bytes 524288 | tf_op jit(solution)/shard_map/jvp(jit(cumsum))/reduce_window_sum | solution.py:38
  162.7 14.1 %all-gather = f32[64,32]{1,0:T(8,128)S(1)} all-gather(f32[8,32]{1,0:T(8,128)S(1)} %get-tuple-element.558), channel_id=2, replica_groups=mesh['sp'=8,'tp'=4] {'sp'}, dimensions={0}, use_global_device_ids=true | all-gather | bytes 9216 | tf_op jit(solution)/shard_map/all_gather | solution.py:15
  180.5 16.9 %all-gather.1 = f32[64,32,64]{2,1,0:T(8,128)S(1)} all-gather(f32[8,32,64]{2,1,0:T(8,128)S(1)} %bitcast.213), channel_id=3, replica_groups=mesh['sp'=8,'tp'=4] {'sp'}, dimensions={0}, use_global_device_ids=true | all-gather | bytes 589824 | tf_op jit(solution)/shard_map/all_gather | solution.py:15
  199.2 5.0 %all-to-all-start.2 = ((bf16[8,80,512]{2,1,0:T(8,128)(2,1)}), bf16[8,80,512]{2,1,0:T(8,128)(2,1)S(1)}, u32[]{:S(2)}, u32[]{:S(2)}) async-start(bf16[8,80,512]{2,1,0:T(8,128)(2,1)} %bitcast.208), calls=%async_computation.3 | async-start | bytes 1310720 | tf_op jit(solution)/shard_map/all_to_all | solution.py:174
  204.6 6.7 %while.63 = (s32[]{:T(128)}, f32[8,32,64]{2,1,0:T(8,128)S(1)}, f32[4,8,32,64]{3,2,1,0:T(8,128)S(1)}, f32[4,8,32]{2,1,0:T(8,128)S(1)}, f32[4,8,32,1]{2,1,3,0:T(8,...) while((s32[]{:T(128)}, f32[8,32,64]{2,1,0:T(8,128)S(1)}, ...), condition=%wide.region_12.13_spmd, body=%wide.region_11.12_spmd.sunk | while | flops 32770 | bytes 477293 | solution.py:51
  230.8 3.1 fusion.20
  234.6 5.0 %fusion.6 = bf16[1,2048,512]{2,1,0:T(8,128)(2,1)} fusion(bf16[640,2048]{1,0:T(8,128)(2,1)} %all-gather.7.cloned.1.call-done, bf16[640,512]{1,0:T(8,128)(2,1)S(1)} %copy-done.28), kind=kOutput, calls=%fused_computation.28 | convolution fusion | flops 1343225856 | bytes 5373952 | tf_op jit(solution)/shard_map/dot_general | solution.py:159
  239.7 3.2 fusion.7
  242.9 3.3 fusion.8
  246.2 11.6 %all-gather.11.cloned.1.call-done = bf16[256,2048]{1,0:T(8,128)(2,1)} async-done(((bf16[256,512]{1,0:T(8,128)(2,1)}), bf16[256,2048]{1,0:T(8,128)(2,1)}) %all-gather.11.cloned.1.call-update) | async-done | bytes 1048592 | tf_op jit(solution)/shard_map/all_gather | solution.py:182
  257.7 3.3 convolution_convert_fusion
  270.8 12.7 %while.65 = (s32[]{:T(128)}, f32[8,32,64]{2,1,0:T(8,128)S(1)}, f32[4,8,32]{2,1,0:T(8,128)S(1)}, f32[4,8,32,64]{3,2,1,0:T(8,128)}, f32[4,8,32,64]{3,2,1,0:T(8,128...) while((s32[]{:T(128)}, f32[8,32,64]{2,1,0:T(8,128)S(1)}, ...), condition=%wide.region_16.17_spmd.clone, body=%wide.region_14.16_spmd.clone.sunk | while | flops 98308 | bytes 472220 | solution.py:51
  286.3 19.8 %all-gather.2 = f32[64,32,64]{2,1,0:T(8,128)} all-gather(f32[8,32,64]{2,1,0:T(8,128)S(1)} %get-tuple-element.402), channel_id=4, replica_groups=mesh['sp'=8,'tp'=4] {'sp'}, dimensions={0}, use_global_device_ids=true | all-gather | bytes 589824 | tf_op jit(solution)/shard_map/all_gather | solution.py:15
  308.3 12.5 %while.66 = (s32[]{:T(128)}, f32[8,32,64]{2,1,0:T(8,128)S(1)}, s32[]{:T(128)}, f32[8,8,32]{2,1,0:T(8,128)}, f32[8,8,32,64]{3,2,1,0:T(8,128)}, /*index=5*/s32[]{:T(128)}, s32[]{:T(128)}) while((s32[]{:T(128)}, f32[8,32,64]{2,1,0:T(8,128)S(1)}, s32[]{:T(128)}, f32[8,8,32]{2,1,0:T(8,128)}, f32[8,8,32,64]{3,2,1,0:T(8,128)}, ...), condition=%wide.region_18.19_spmd.clone, body=%wide.region_17.18_spmd.clone.sunk | while | flops 65540 | bytes 199793 | solution.py:27
  327.1 2.9 pad_add_fusion.1
  349.0 25.7 %fusion.67 = f32[4,64,8,32]{3,2,1,0:T(8,128)S(1)} fusion(f32[4,64,8,32]{3,2,1,0:T(8,128)S(1)} %copy.145), kind=kOutput, calls=%fused_computation.147 | output fusion | flops 4128768 | bytes 524288 | tf_op jit(solution)/shard_map/transpose(jvp(jit(cumsum)))/reduce_window_sum | solution.py:38
  374.7 25.8 %fusion.68 = f32[4,64,8,32]{3,2,1,0:T(8,128)S(1)} fusion(f32[4,64,8,32]{3,2,1,0:T(8,128)S(1)} %copy-done.16), kind=kOutput, calls=%fused_computation.148 | output fusion | flops 4128768 | bytes 524288 | tf_op jit(solution)/shard_map/transpose(jvp(jit(cumsum)))/reduce_window_sum | solution.py:62
  (289 shorter events, 128.4 us)
Async XLA Ops:
  7.2 73.8 %copy-start = (bf16[1,2048,512]{2,1,0:T(8,128)(2,1)S(1)}, bf16[1,2048,512]{2,1,0:T(8,128)(2,1)}, u32[]{:S(2)}) copy-start(bf16[1,2048,512]{2,1,0:T(8,128)(2,1)} %param.24) | copy-start | bytes 6291460
  7.2 73.8 %all-gather.7.cloned.1.call-start = ((), (), s32[]{:S(2)}) async-start(), calls=%async_computation.5 | async-start | bytes 3276800 | tf_op jit(solution)/shard_map/all_gather | solution.py:138
  17.9 24.6 %copy-start.26 = (bf16[256,512]{1,0:T(8,128)(2,1)S(1)}, bf16[256,512]{1,0:T(8,128)(2,1)}, u32[]{:S(2)}) copy-start(bf16[256,512]{1,0:T(8,128)(2,1)} %param.21) | copy-start | bytes 786436
  42.5 79.7 %all-gather.9.cloned.1.call-start = ((), (), s32[]{:S(2)}) async-start(), calls=%async_computation.6 | async-start | bytes 3276800 | tf_op jit(solution)/shard_map/all_gather | solution.py:139
  70.6 128.7 %reduce-scatter.3.cloned.1.call-start = ((), (), s32[]{:S(2)}) async-start(), calls=%async_computation.7 | async-start | bytes 3276800 | tf_op jit(solution)/shard_map/reduce_scatter | solution.py:171
  84.4 37.8 %copy-start.50 = (f32[640,512]{1,0:T(8,128)}, f32[640,512]{1,0:T(8,128)S(1)}, u32[]{:S(2)}) copy-start(f32[640,512]{1,0:T(8,128)S(1)} %fusion.11) | copy-start | bytes 3932164
  133.6 26.3 %copy-start.39 = (bf16[256,256]{1,0:T(8,128)(2,1)S(1)}, bf16[256,256]{1,0:T(8,128)(2,1)}, u32[]{:S(2)}) copy-start(bf16[256,256]{1,0:T(8,128)(2,1)} %param.28) | copy-start | bytes 393220
  159.9 59.2 %copy-start.2 = (f32[4,64,8,32]{1,3,2,0:T(8,128)}, f32[4,64,8,32]{1,3,2,0:T(8,128)S(1)}, u32[]{:S(2)}) copy-start(f32[4,64,8,32]{1,3,2,0:T(8,128)S(1)} %copy.122) | copy-start | bytes 786436
  160.7 17.6 %copy-start.12 = (f32[4,64,8,32]{1,0,3,2:T(4,128)}, f32[4,64,8,32]{1,0,3,2:T(4,128)S(1)}, u32[]{:S(2)}) copy-start(f32[4,64,8,32]{1,0,3,2:T(4,128)S(1)} %reshape.242) | copy-start | bytes 786436
  161.8 16.6 %copy-start.41 = (f32[8,32]{1,0:T(8,128)}, f32[8,32]{1,0:T(8,128)S(1)}, u32[]{:S(2)}) copy-start(f32[8,32]{1,0:T(8,128)S(1)} %get-tuple-element.558) | copy-start | bytes 3076
  162.5 15.8 %copy-start.31 = (f32[4,8,32]{2,1,0:T(8,128)}, f32[4,8,32]{2,1,0:T(8,128)S(1)}, u32[]{:S(2)}) copy-start(f32[4,8,32]{2,1,0:T(8,128)S(1)} %fusion.25) | copy-start | bytes 12292
  199.2 5.1 %copy-start.10 = (f32[8,32,64]{2,1,0:T(8,128)}, f32[8,32,64]{2,1,0:T(8,128)S(1)}, u32[]{:S(2)}) copy-start(f32[8,32,64]{2,1,0:T(8,128)S(1)} %get-tuple-element.750) | copy-start | bytes 196612
  199.2 25.0 %all-to-all-start.2 = ((bf16[8,80,512]{2,1,0:T(8,128)(2,1)}), bf16[8,80,512]{2,1,0:T(8,128)(2,1)S(1)}, u32[]{:S(2)}, u32[]{:S(2)}) async-start(bf16[8,80,512]{2,1,0:T(8,128)(2,1)} %bitcast.208), calls=%async_computation.3 | async-start | bytes 1310720 | tf_op jit(solution)/shard_map/all_to_all | solution.py:174
  204.3 7.0 %copy-start.44 = (s32[512]{0:T(512)S(1)}, s32[512]{0:T(512)}, u32[]{:S(2)}) copy-start(s32[512]{0:T(512)} %copy-done.43) | copy-start | bytes 6148
  204.3 53.4 %all-gather.11.cloned.1.call-start = ((), (), s32[]{:S(2)}) async-start(), calls=%async_computation.8 | async-start | bytes 1310720 | tf_op jit(solution)/shard_map/all_gather | solution.py:182
  211.3 19.5 %copy-start.4 = (f32[4,8,32,64]{3,2,1,0:T(8,128)}, f32[4,8,32,64]{3,2,1,0:T(8,128)S(1)}, u32[]{:S(2)}) copy-start(f32[4,8,32,64]{3,2,1,0:T(8,128)S(1)} %get-tuple-element.779) | copy-start | bytes 786436
  230.7 170.9 %reduce-scatter.5.cloned.1.call-start = ((), (), s32[]{:S(2)}) async-start(), calls=%async_computation.9 | async-start | bytes 2359296 | tf_op jit(solution)/shard_map/reduce_scatter | solution.py:183
  270.8 12.7 %copy-start.3 = (f32[4,64,8,32]{1,3,2,0:T(8,128)S(1)}, f32[4,64,8,32]{1,3,2,0:T(8,128)}, u32[]{:S(2)}) copy-start(f32[4,64,8,32]{1,3,2,0:T(8,128)} %copy-done.2) | copy-start | bytes 786436
  306.0 15.8 %copy-start.32 = (f32[4,8,32]{2,1,0:T(8,128)S(1)}, f32[4,8,32]{2,1,0:T(8,128)}, u32[]{:S(2)}) copy-start(f32[4,8,32]{2,1,0:T(8,128)} %copy-done.31) | copy-start | bytes 12292
  330.0 6.8 %copy-start.9 = (f32[4,64,8,32]{1,3,2,0:T(8,128)S(1)}, f32[4,64,8,32]{1,3,2,0:T(8,128)}, u32[]{:S(2)}) copy-start(f32[4,64,8,32]{1,3,2,0:T(8,128)} %copy-done.8) | copy-start | bytes 786436
  330.0 6.8 %copy-start.14 = (f32[4,8,32,64]{3,2,1,0:T(8,128)S(1)}, f32[4,8,32,64]{3,2,1,0:T(8,128)}, u32[]{:S(2)}) copy-start(f32[4,8,32,64]{3,2,1,0:T(8,128)} %get-tuple-element.401) | copy-start | bytes 786436
  330.9 7.8 %copy-start.7 = (f32[4,8,64,64]{3,2,1,0:T(8,128)S(1)}, f32[4,8,64,64]{3,2,1,0:T(8,128)}, u32[]{:S(2)}) copy-start(f32[4,8,64,64]{3,2,1,0:T(8,128)} %copy-done.6) | copy-start | bytes 1572868
  349.0 25.7 %copy-start.16 = (f32[4,64,8,32]{3,2,1,0:T(8,128)S(1)}, f32[4,64,8,32]{3,2,1,0:T(8,128)}, u32[]{:S(2)}) copy-start(f32[4,64,8,32]{3,2,1,0:T(8,128)} %copy.149) | copy-start | bytes 786436
  374.7 28.7 %copy-start.1 = (bf16[1,2048,512]{2,1,0:T(8,128)(2,1)S(1)}, bf16[1,2048,512]{2,1,0:T(8,128)(2,1)}, u32[]{:S(2)}) copy-start(bf16[1,2048,512]{2,1,0:T(8,128)(2,1)} %param.24) | copy-start | bytes 6291460
  (35 other events, 82.3 us)
Sparse Core Ops, SparseCore 0:
  42.6 38.3 all-gather.6
  82.8 39.3 all-gather.8
  132.2 39.5 reduce-scatter.2
  230.8 26.8 all-gather.10
  261.2 36.9 reduce-scatter.4
where the time goes:
time: 417 us; the launch traced here: 410 us
  other arithmetic  115 us (28%)
  blocking collectives  96.4 us (23%)
  matrix products  62.1 us (15%)
  local copies, waits for them, and re-layouts  58.6 us (14%)
  waiting for transfers between devices  56.7 us (14%)
  between operations  15.2 us (4%)
  starting transfers between devices  5.94 us (1%)
    another operation x2, other arithmetic, mixer_pass(): cumulative = jnp.cumsum(decays, axis=1)  51.5 us
    all_gather x3, blocking collectives, carried_in(): pieces = jax.tree.map(lambda part: lax.all_gather(part, axis), value)  50.8 us
    all_gather x1, waiting for transfers between devices, body(): lax.all_gather(recv_grad.reshape(row_total, -1), 'tp', axis=1, tiled=True)  35.2 us
    another operation x1, other arithmetic, carry_terms(): jnp.cumsum(decay_full.reshape(blocks, BLOCK, nheads, KEY_CHANNELS), axis=1)  25.8 us
    all_to_all x1, blocking collectives, body(): lax.all_to_all(send_in, 'sp', split_axis=0, concat_axis=0, tiled=True)  24.4 us
    all_to_all x1, blocking collectives, body(): lax.all_to_all(send_grad, 'sp', split_axis=0, concat_axis=0, tiled=True)  21.2 us
    all_gather x1, waiting for transfers between devices, body(): full_grad = lax.all_gather(residual_grad, 'tp', axis=1, tiled=True)  11.6 us
    all_gather x1, waiting for transfers between devices, body(): lax.all_gather(recv_in.reshape(row_total, -1), 'tp', axis=1, tiled=True)  9.84 us
  transfers between devices with their start and end apart: 6, of which 3 were waited for; matrix products, arithmetic and copies ran while one was open for 48% of the time, Pallas kernels for 0%

commit v1 on v0

--- a/solution.py
+++ b/solution.py
@@ -136,7 +136,15 @@
     )
     rows_in, rows_grad = (
         lax.all_gather(recv_in.reshape(row_total, -1), "tp", axis=1, tiled=True),
-        lax.all_gather(recv_grad.reshape(row_total, -1), "tp", axis=1, tiled=True),
+        jnp.concatenate(
+            lax.all_to_all(
+                jnp.stack(lax.axis_size("tp") * [recv_grad.reshape(row_total, -1)], axis=0),
+                "tp",
+                0,
+                0,
+            ),
+            axis=1,
+        ),
     )
     gate_weight = w_gate[0]
     up_weight = w_up[0]

time: 417 us -> 404 us (0.969)
  waiting for transfers between devices: 56.7 us -> 36 us
  starting transfers between devices: 5.94 us -> 10.3 us
    all_gather x1 -> x0, waiting for transfers between devices: 35.2 us -> none  [body(): lax.all_gather(recv_grad.reshape(row_total, -1), 'tp', axis=1, tiled=True)]
    all_gather x1, waiting for transfers between devices: 9.84 us -> 19.9 us  [body(): lax.all_gather(recv_in.reshape(row_total, -1), 'tp', axis=1, tiled=True)]
    all_to_all x0 -> x1, waiting for transfers between devices: none -> 6.12 us  [body(): lax.all_to_all(jnp.stack(lax.axis_size('tp') * [recv_grad.reshape(row_tot...]
    all_to_all x0 -> x1, starting transfers between devices: none -> 4.56 us  [body(): lax.all_to_all(jnp.stack(lax.axis_size('tp') * [recv_grad.reshape(row_tot...]
    unnamed x111 -> x109, local copies, waits for them, and re-layouts: 9.22 us -> 9.23 us
  transfers between devices with their start and end apart: 6 -> 6, of which waited for: 3 -> 3; matrix products, arithmetic and copies ran while one was open for 48% -> 51% of each run, Pallas kernels for 0% -> 0%
where the time goes in v1:
time: 404 us; the launch traced here: 397 us
  other arithmetic  115 us (28%)
  blocking collectives  95.8 us (24%)
  matrix products  63.8 us (16%)
  local copies, waits for them, and re-layouts  60.6 us (15%)
  waiting for transfers between devices  36 us (9%)
  between operations  15.2 us (4%)
  starting transfers between devices  10.3 us (3%)
    another operation x2, other arithmetic, mixer_pass(): cumulative = jnp.cumsum(decays, axis=1)  51.5 us
    all_gather x3, blocking collectives, carried_in(): pieces = jax.tree.map(lambda part: lax.all_gather(part, axis), value)  50.9 us
    another operation x1, other arithmetic, carry_terms(): jnp.cumsum(decay_full.reshape(blocks, BLOCK, nheads, KEY_CHANNELS), axis=1)  25.8 us
    all_to_all x1, blocking collectives, body(): lax.all_to_all(send_in, 'sp', split_axis=0, concat_axis=0, tiled=True)  24.4 us
    all_to_all x1, blocking collectives, body(): lax.all_to_all(send_grad, 'sp', split_axis=0, concat_axis=0, tiled=True)  20.5 us
    all_gather x1, waiting for transfers between devices, body(): lax.all_gather(recv_in.reshape(row_total, -1), 'tp', axis=1, tiled=True)  19.9 us
    all_gather x1, waiting for transfers between devices, body(): full_grad = lax.all_gather(residual_grad, 'tp', axis=1, tiled=True)  9.91 us
    unnamed x109, local copies, waits for them, and re-layouts  9.23 us
  transfers between devices with their start and end apart: 6, of which 3 were waited for; matrix products, arithmetic and copies ran while one was open for 51% of the time, Pallas kernels for 0%

profile of v1, /device:TPU:0, one launch (start us, length us, event | category | flops | bytes accessed | tf_op | source)
XLA Modules:
  0.0 397.1 jit_solution(12184053926959064230)
XLA Ops:
  18.1 24.4 %all_to_all.20 = bf16[8,80,512]{2,1,0:T(8,128)(2,1)} all-to-all(bf16[8,80,512]{2,1,0:T(8,128)(2,1)S(1)} %broadcast_select_fusion.2), channel_id=1, replica_groups=mesh['sp'=8,'tp'=4] {'sp'}, dimensions={0} | all-to-all | bytes 1310720 | tf_op jit(solution)/shard_map/all_to_all | solution.py:134
  49.2 20.5 %all_to_all.21 = bf16[8,80,512]{2,1,0:T(8,128)(2,1)S(1)} all-to-all(bf16[8,80,512]{2,1,0:T(8,128)(2,1)S(1)} %broadcast_select_fusion.1), channel_id=1, replica_groups=mesh['sp'=8,'tp'=4] {'sp'}, dimensions={0} | all-to-all | bytes 1310720 | tf_op jit(solution)/shard_map/all_to_all | solution.py:135
  71.8 4.6 %all-to-all-start.2 = ((bf16[4,640,512]{1,2,0:T(8,128)(2,1)}), bf16[4,640,512]{1,2,0:T(8,128)(2,1)}, u32[]{:S(2)}, u32[]{:S(2)}) async-start(bf16[4,640,512]{1,2,0:T(8,128)(2,1)} %stack.3), calls=%async_computation.2 | async-start | bytes 5242880 | tf_op jit(solution)/shard_map/all_to_all | solution.py:140
  76.9 19.9 %all-gather.6.cloned.1.call-done = bf16[640,2048]{1,0:T(8,128)(2,1)} async-done(((bf16[640,512]{1,0:T(8,128)(2,1)}), bf16[640,2048]{1,0:T(8,128)(2,1)}) %all-gather.6.cloned.1.call-update) | async-done | bytes 2621456 | tf_op jit(solution)/shard_map/all_gather | solution.py:138
  96.8 3.4 fusion.11
  102.8 6.1 %all-to-all-done.2 = bf16[4,640,512]{1,2,0:T(8,128)(2,1)} async-done(((bf16[4,640,512]{1,2,0:T(8,128)(2,1)}), bf16[4,640,512]{1,2,0:T(8,128)(2,1)}, u32[]{:S(2)}, u32[]{:S(2)}) %all-to-all-start.2) | async-done | bytes 2621472 | tf_op jit(solution)/shard_map/all_to_all | solution.py:140
  108.9 4.7 %multiply_convert_fusion.1 = (bf16[640,512]{1,0:T(8,128)(2,1)S(1)}, bf16[640,512]{1,0:T(8,128)(2,1)S(1)}) fusion(f32[640,512]{1,0:T(8,128)S(1)} %fusion.11, f32[640,512]{1,0:T(8,128)} %fusion.14, bf16[640,2048]{0,1:T(8,128)(2,1)} %bitcast.13, bf16[1,512,2048]{2,1,0:T(8,128)(2,1)} %param.26), kind=kOutput, calls=%fused_computation.48 | convolution fusion | flops 1346437120 | bytes 8650752 | tf_op jit(solution)/shard_map/dot_general | solution.py:157
  115.7 3.1 add_convert_fusion
  120.4 25.9 %fusion.66 = f32[4,64,8,32]{3,2,1,0:T(8,128)S(1)} fusion(f32[4,64,8,32]{3,2,1,0:T(8,128)S(1)} %reshape.290), kind=kOutput, calls=%fused_computation.146 | output fusion | flops 4128768 | bytes 524288 | tf_op jit(solution)/shard_map/jvp(jit(cumsum))/reduce_window_sum | solution.py:38
  149.4 14.1 %all-gather = f32[64,32]{1,0:T(8,128)S(1)} all-gather(f32[8,32]{1,0:T(8,128)S(1)} %get-tuple-element.558), channel_id=2, replica_groups=mesh['sp'=8,'tp'=4] {'sp'}, dimensions={0}, use_global_device_ids=true | all-gather | bytes 9216 | tf_op jit(solution)/shard_map/all_gather | solution.py:15
  167.2 17.0 %all-gather.1 = f32[64,32,64]{2,1,0:T(8,128)S(1)} all-gather(f32[8,32,64]{2,1,0:T(8,128)S(1)} %bitcast.216), channel_id=3, replica_groups=mesh['sp'=8,'tp'=4] {'sp'}, dimensions={0}, use_global_device_ids=true | all-gather | bytes 589824 | tf_op jit(solution)/shard_map/all_gather | solution.py:15
  186.2 5.0 %all-to-all-start.3 = ((bf16[8,80,512]{2,1,0:T(8,128)(2,1)}), bf16[8,80,512]{2,1,0:T(8,128)(2,1)S(1)}, u32[]{:S(2)}, u32[]{:S(2)}) async-start(bf16[8,80,512]{2,1,0:T(8,128)(2,1)} %bitcast.211), calls=%async_computation.4 | async-start | bytes 1310720 | tf_op jit(solution)/shard_map/all_to_all | solution.py:182
  191.3 6.7 %while.63 = (s32[]{:T(128)}, f32[8,32,64]{2,1,0:T(8,128)S(1)}, f32[4,8,32,64]{3,2,1,0:T(8,128)S(1)}, f32[4,8,32]{2,1,0:T(8,128)S(1)}, f32[4,8,32,1]{2,1,3,0:T(8,...) while((s32[]{:T(128)}, f32[8,32,64]{2,1,0:T(8,128)S(1)}, ...), condition=%wide.region_12.13_spmd, body=%wide.region_11.12_spmd.sunk | while | flops 32770 | bytes 477293 | solution.py:51
  217.6 3.1 fusion.20
  221.4 5.0 %fusion.6 = bf16[1,2048,512]{2,1,0:T(8,128)(2,1)} fusion(bf16[640,2048]{1,0:T(8,128)(2,1)} %all-gather.6.cloned.1.call-done, bf16[640,512]{1,0:T(8,128)(2,1)S(1)} %copy-done.28), kind=kOutput, calls=%fused_computation.28 | convolution fusion | flops 1343225856 | bytes 5373952 | tf_op jit(solution)/shard_map/dot_general | solution.py:167
  226.5 3.2 fusion.7
  229.6 4.9 %fusion.8 = bf16[1,512,2048]{2,1,0:T(8,128)(2,1)} fusion(bf16[640,2048]{0,1:T(8,128)(2,1)} %bitcast.13, f32[640,512]{1,0:T(8,128)S(1)} %copy-done.51, f32[640,512]{1,0:T(8,128)S(1)} %copy-done.50), kind=kOutput, calls=%fused_computation.30 | convolution fusion | flops 1345191936 | bytes 7340032 | tf_op jit(solution)/shard_map/dot_general | solution.py:160
  234.6 9.9 %all-gather.8.cloned.1.call-done = bf16[256,2048]{1,0:T(8,128)(2,1)} async-done(((bf16[256,512]{1,0:T(8,128)(2,1)}), bf16[256,2048]{1,0:T(8,128)(2,1)}) %all-gather.8.cloned.1.call-update) | async-done | bytes 1048592 | tf_op jit(solution)/shard_map/all_gather | solution.py:190
  244.5 3.3 convolution_convert_fusion
  257.6 12.7 %while.65 = (s32[]{:T(128)}, f32[8,32,64]{2,1,0:T(8,128)S(1)}, f32[4,8,32]{2,1,0:T(8,128)S(1)}, f32[4,8,32,64]{3,2,1,0:T(8,128)}, f32[4,8,32,64]{3,2,1,0:T(8,128...) while((s32[]{:T(128)}, f32[8,32,64]{2,1,0:T(8,128)S(1)}, ...), condition=%wide.region_16.17_spmd.clone, body=%wide.region_14.16_spmd.clone.sunk | while | flops 98308 | bytes 472220 | solution.py:51
  273.0 19.8 %all-gather.2 = f32[64,32,64]{2,1,0:T(8,128)} all-gather(f32[8,32,64]{2,1,0:T(8,128)S(1)} %get-tuple-element.402), channel_id=4, replica_groups=mesh['sp'=8,'tp'=4] {'sp'}, dimensions={0}, use_global_device_ids=true | all-gather | bytes 589824 | tf_op jit(solution)/shard_map/all_gather | solution.py:15
  295.1 12.5 %while.66 = (s32[]{:T(128)}, f32[8,32,64]{2,1,0:T(8,128)S(1)}, s32[]{:T(128)}, f32[8,8,32]{2,1,0:T(8,128)}, f32[8,8,32,64]{3,2,1,0:T(8,128)}, /*index=5*/s32[]{:T(128)}, s32[]{:T(128)}) while((s32[]{:T(128)}, f32[8,32,64]{2,1,0:T(8,128)S(1)}, s32[]{:T(128)}, f32[8,8,32]{2,1,0:T(8,128)}, f32[8,8,32,64]{3,2,1,0:T(8,128)}, ...), condition=%wide.region_18.19_spmd.clone, body=%wide.region_17.18_spmd.clone.sunk | while | flops 65540 | bytes 199793 | solution.py:27
  335.8 25.7 %fusion.67 = f32[4,64,8,32]{3,2,1,0:T(8,128)S(1)} fusion(f32[4,64,8,32]{3,2,1,0:T(8,128)S(1)} %copy.148), kind=kOutput, calls=%fused_computation.147 | output fusion | flops 4128768 | bytes 524288 | tf_op jit(solution)/shard_map/transpose(jvp(jit(cumsum)))/reduce_window_sum | solution.py:38
  361.5 25.8 %fusion.68 = f32[4,64,8,32]{3,2,1,0:T(8,128)S(1)} fusion(f32[4,64,8,32]{3,2,1,0:T(8,128)S(1)} %copy-done.16), kind=kOutput, calls=%fused_computation.148 | output fusion | flops 4128768 | bytes 524288 | tf_op jit(solution)/shard_map/transpose(jvp(jit(cumsum)))/reduce_window_sum | solution.py:62
  (288 shorter events, 133.0 us)
Async XLA Ops:
  7.2 89.6 %copy-start = (bf16[1,2048,512]{2,1,0:T(8,128)(2,1)S(1)}, bf16[1,2048,512]{2,1,0:T(8,128)(2,1)}, u32[]{:S(2)}) copy-start(bf16[1,2048,512]{2,1,0:T(8,128)(2,1)} %param.24) | copy-start | bytes 6291460
  7.2 89.6 %all-gather.6.cloned.1.call-start = ((), (), s32[]{:S(2)}) async-start(), calls=%async_computation.6 | async-start | bytes 3276800 | tf_op jit(solution)/shard_map/all_gather | solution.py:138
  17.9 24.6 %copy-start.26 = (bf16[256,512]{1,0:T(8,128)(2,1)S(1)}, bf16[256,512]{1,0:T(8,128)(2,1)}, u32[]{:S(2)}) copy-start(bf16[256,512]{1,0:T(8,128)(2,1)} %param.21) | copy-start | bytes 786436
  71.8 37.2 %all-to-all-start.2 = ((bf16[4,640,512]{1,2,0:T(8,128)(2,1)}), bf16[4,640,512]{1,2,0:T(8,128)(2,1)}, u32[]{:S(2)}, u32[]{:S(2)}) async-start(bf16[4,640,512]{1,2,0:T(8,128)(2,1)} %stack.3), calls=%async_computation.2 | async-start | bytes 5242880 | tf_op jit(solution)/shard_map/all_to_all | solution.py:140
  76.3 109.8 %reduce-scatter.3.cloned.1.call-start = ((), (), s32[]{:S(2)}) async-start(), calls=%async_computation.7 | async-start | bytes 3276800 | tf_op jit(solution)/shard_map/reduce_scatter | solution.py:179
  100.2 8.7 %copy-start.49 = (f32[640,512]{1,0:T(8,128)}, f32[640,512]{1,0:T(8,128)S(1)}, u32[]{:S(2)}) copy-start(f32[640,512]{1,0:T(8,128)S(1)} %fusion.11) | copy-start | bytes 3932164
  120.4 26.3 %copy-start.39 = (bf16[256,256]{1,0:T(8,128)(2,1)S(1)}, bf16[256,256]{1,0:T(8,128)(2,1)}, u32[]{:S(2)}) copy-start(bf16[256,256]{1,0:T(8,128)(2,1)} %param.28) | copy-start | bytes 393220
  146.6 59.2 %copy-start.2 = (f32[4,64,8,32]{1,3,2,0:T(8,128)}, f32[4,64,8,32]{1,3,2,0:T(8,128)S(1)}, u32[]{:S(2)}) copy-start(f32[4,64,8,32]{1,3,2,0:T(8,128)S(1)} %copy.125) | copy-start | bytes 786436
  147.5 17.6 %copy-start.12 = (f32[4,64,8,32]{1,0,3,2:T(4,128)}, f32[4,64,8,32]{1,0,3,2:T(4,128)S(1)}, u32[]{:S(2)}) copy-start(f32[4,64,8,32]{1,0,3,2:T(4,128)S(1)} %reshape.248) | copy-start | bytes 786436
  148.6 16.6 %copy-start.41 = (f32[8,32]{1,0:T(8,128)}, f32[8,32]{1,0:T(8,128)S(1)}, u32[]{:S(2)}) copy-start(f32[8,32]{1,0:T(8,128)S(1)} %get-tuple-element.558) | copy-start | bytes 3076
  149.3 15.8 %copy-start.31 = (f32[4,8,32]{2,1,0:T(8,128)}, f32[4,8,32]{2,1,0:T(8,128)S(1)}, u32[]{:S(2)}) copy-start(f32[4,8,32]{2,1,0:T(8,128)S(1)} %fusion.25) | copy-start | bytes 12292
  186.1 5.1 %copy-start.10 = (f32[8,32,64]{2,1,0:T(8,128)}, f32[8,32,64]{2,1,0:T(8,128)S(1)}, u32[]{:S(2)}) copy-start(f32[8,32,64]{2,1,0:T(8,128)S(1)} %get-tuple-element.750) | copy-start | bytes 196612
  186.2 24.9 %all-to-all-start.3 = ((bf16[8,80,512]{2,1,0:T(8,128)(2,1)}), bf16[8,80,512]{2,1,0:T(8,128)(2,1)S(1)}, u32[]{:S(2)}, u32[]{:S(2)}) async-start(bf16[8,80,512]{2,1,0:T(8,128)(2,1)} %bitcast.211), calls=%async_computation.4 | async-start | bytes 1310720 | tf_op jit(solution)/shard_map/all_to_all | solution.py:182
  191.2 6.9 %copy-start.44 = (s32[512]{0:T(512)S(1)}, s32[512]{0:T(512)}, u32[]{:S(2)}) copy-start(s32[512]{0:T(512)} %copy-done.43) | copy-start | bytes 6148
  191.2 53.3 %all-gather.8.cloned.1.call-start = ((), (), s32[]{:S(2)}) async-start(), calls=%async_computation.8 | async-start | bytes 1310720 | tf_op jit(solution)/shard_map/all_gather | solution.py:190
  198.1 19.5 %copy-start.4 = (f32[4,8,32,64]{3,2,1,0:T(8,128)}, f32[4,8,32,64]{3,2,1,0:T(8,128)S(1)}, u32[]{:S(2)}) copy-start(f32[4,8,32,64]{3,2,1,0:T(8,128)S(1)} %get-tuple-element.779) | copy-start | bytes 786436
  217.5 170.9 %reduce-scatter.5.cloned.1.call-start = ((), (), s32[]{:S(2)}) async-start(), calls=%async_computation.9 | async-start | bytes 2359296 | tf_op jit(solution)/shard_map/reduce_scatter | solution.py:191
  257.6 12.7 %copy-start.3 = (f32[4,64,8,32]{1,3,2,0:T(8,128)S(1)}, f32[4,64,8,32]{1,3,2,0:T(8,128)}, u32[]{:S(2)}) copy-start(f32[4,64,8,32]{1,3,2,0:T(8,128)} %copy-done.2) | copy-start | bytes 786436
  292.8 15.8 %copy-start.32 = (f32[4,8,32]{2,1,0:T(8,128)S(1)}, f32[4,8,32]{2,1,0:T(8,128)}, u32[]{:S(2)}) copy-start(f32[4,8,32]{2,1,0:T(8,128)} %copy-done.31) | copy-start | bytes 12292
  316.8 6.8 %copy-start.9 = (f32[4,64,8,32]{1,3,2,0:T(8,128)S(1)}, f32[4,64,8,32]{1,3,2,0:T(8,128)}, u32[]{:S(2)}) copy-start(f32[4,64,8,32]{1,3,2,0:T(8,128)} %copy-done.8) | copy-start | bytes 786436
  316.8 6.8 %copy-start.14 = (f32[4,8,32,64]{3,2,1,0:T(8,128)S(1)}, f32[4,8,32,64]{3,2,1,0:T(8,128)}, u32[]{:S(2)}) copy-start(f32[4,8,32,64]{3,2,1,0:T(8,128)} %get-tuple-element.401) | copy-start | bytes 786436
  317.7 7.8 %copy-start.7 = (f32[4,8,64,64]{3,2,1,0:T(8,128)S(1)}, f32[4,8,64,64]{3,2,1,0:T(8,128)}, u32[]{:S(2)}) copy-start(f32[4,8,64,64]{3,2,1,0:T(8,128)} %copy-done.6) | copy-start | bytes 1572868
  335.8 25.7 %copy-start.16 = (f32[4,64,8,32]{3,2,1,0:T(8,128)S(1)}, f32[4,64,8,32]{3,2,1,0:T(8,128)}, u32[]{:S(2)}) copy-start(f32[4,64,8,32]{3,2,1,0:T(8,128)} %copy.152) | copy-start | bytes 786436
  361.5 28.7 %copy-start.1 = (bf16[1,2048,512]{2,1,0:T(8,128)(2,1)S(1)}, bf16[1,2048,512]{2,1,0:T(8,128)(2,1)}, u32[]{:S(2)}) copy-start(bf16[1,2048,512]{2,1,0:T(8,128)(2,1)} %param.24) | copy-start | bytes 6291460
  (34 other events, 79.1 us)
Sparse Core Ops, SparseCore 0:
  42.6 54.1 all-gather.5
  118.9 39.5 reduce-scatter.2
  217.6 26.8 all-gather.7
  248.0 36.9 reduce-scatter.4
